TPU v7x, 256 devices: a whole 4x4x8 slice. The times are simulated.
256 devices in a mesh: ep: 64 (over z, y, core), tp: 4 (over x).
Axes of the slice: x: 4, y: 4, z: 8, core: 2. Of those that a mesh axis runs over, the one named last changes fastest.
Arguments:
- tokens: bfloat16 [16384, 2048], P('ep'), may hold values from -6 to 6
- norm_gain: float32 [2048], replicated, may hold values from 0.1 to 1.9
- expert_ids: int32 [16384, 2], P('ep'), may hold values from 0 to 31, all different within a row; in each aligned block of 256 rows (0 to 255, 256 to 511, ...) at most 20 rows name the same one
- route_weight: float32 [16384, 2], P('ep'), may hold values from 0.2 to 1
- w_gate: bfloat16 [64, 2048, 3584], P('ep', None, 'tp'), may hold values from -0.125 to 0.125
- w_up: bfloat16 [64, 2048, 3584], P('ep', None, 'tp'), may hold values from -0.125 to 0.125
- w_down: bfloat16 [64, 3584, 2048], P('ep', 'tp'), may hold values from -0.0625 to 0.0625
Outputs:
- mixed: bfloat16 [16384, 2048], P('ep', 'tp')
Inputs may be any that keep to these rules, and one draw needn't show every extreme that they name: `expert_ids`: A token names 2 different experts. In each aligned block of 256 tokens (the tokens of one index of ep) no expert is named by more than 20 tokens, a bound that some block reaches.
All inputs are finite; a program needn't handle non-finite values.
Results may differ from a plain program's by a relative error of at most 0.014.
Values may be sent and summed in bfloat16 or wider, within the bound.
No kernel may reach another device: no remote copies, remote signals or barrier semaphores. Data moves between devices by JAX's collectives and lax.ppermute only.
A program may use at most 128 MiB of HBM per device.

v0:
```python
import jax
import jax.numpy as jnp
from jax import lax
from jax.sharding import Mesh
from jax.sharding import PartitionSpec as P

HALVES = 2
EP = ("ep_0", "ep_1", "ep_2")


EPSILON = 1e-05


def split_up(array, dim, count):
    lengths = array.shape
    parts = array.reshape(*lengths[:dim], count, lengths[dim] // count, *lengths[dim + 1 :])
    return jnp.moveaxis(parts, dim, 0)


def in_order(parts, dim):
    parts = jnp.moveaxis(parts, 0, dim)
    lengths = parts.shape
    return parts.reshape(*lengths[:dim], lengths[dim] * lengths[dim + 1], *lengths[dim + 2 :])


def exchange_in_order(parts, axes, order):
    inside = parts.shape[1:]
    out = parts.reshape(*(lax.axis_size(a) for a in axes), *inside)
    for k in order:
        out = lax.all_to_all(out, axes[k], k, k, tiled=True)
    return out.reshape(-1, *inside)


def two_step_exchange(array, groups, order, split_dim, concat_dim):
    count = lax.axis_size(groups[0]) * lax.axis_size(groups[1])
    parts = split_up(array, split_dim, count)
    return in_order(exchange_in_order(parts, groups, order), concat_dim)


def swapped(value, axis, distance):
    mask = 2**distance
    pairs = [(source, source ^ mask) for source in range(lax.axis_size(axis))]
    return lax.ppermute(value, axis, pairs)


def sent_and_summed(array, axis, dim):
    count = lax.axis_size(axis)
    parts = lax.all_to_all(split_up(array, dim, count), axis, 0, 0, tiled=True)
    return jnp.sum(parts.astype(jnp.float32), axis=0)


def layer_normed(tokens, norm_gain):
    values = tokens.astype(jnp.float32)
    center = values - jnp.mean(values, axis=-1, keepdims=True)
    spread = jnp.mean(center * center, axis=-1, keepdims=True)
    return (center * lax.rsqrt(spread + EPSILON) * norm_gain).astype(jnp.bfloat16)


def slot_numbers(chosen, experts):
    onehot = (chosen[..., None] == jnp.arange(experts, dtype=jnp.int32)).astype(jnp.int32)
    before = jnp.cumsum(onehot, axis=1) - onehot
    return jnp.sum(before * onehot, axis=-1)


def body(tokens, norm_gain, expert_ids, route_weight, w_gate, w_up, w_down):
    tok_rows, width = tokens.shape
    top_count = expert_ids.shape[1]
    ep_count = lax.axis_size(EP)
    experts = ep_count // HALVES
    capacity = 2 * min(tok_rows // 2, 5 * tok_rows * top_count // (8 * experts))
    normed = layer_normed(tokens, norm_gain)
    padded = jnp.concatenate([normed, jnp.zeros((1, width), jnp.bfloat16)], axis=0)
    slots = slot_numbers(expert_ids.reshape(1, -1), experts).reshape(-1)
    flat_expert = expert_ids.reshape(-1)
    owner = jnp.arange(tok_rows * top_count, dtype=jnp.int32) // top_count
    place = flat_expert * capacity + slots
    table = jnp.full((experts * capacity,), tok_rows, jnp.int32).at[place].set(owner)
    outgoing = padded[table].reshape(experts, capacity, width)
    halved = outgoing.reshape(experts * HALVES, capacity // HALVES, width)
    mine = two_step_exchange(halved, (("ep_0", "ep_1"), "ep_2"), (0, 1), 0, 0)
    other = swapped(mine, EP, 0)
    is_first = lax.axis_index(EP) % 2 == 0
    leading = jnp.where(is_first, mine, other)
    trailing = jnp.where(is_first, other, mine)
    arrived = jnp.concatenate([leading, trailing], axis=1)
    routed = arrived.reshape(-1, width)
    gate = jnp.dot(routed, w_gate[0], preferred_element_type=jnp.float32)
    up = jnp.dot(routed, w_up[0], preferred_element_type=jnp.float32)
    hidden = (jax.nn.silu(gate) * up).astype(jnp.bfloat16)
    partial_value = jnp.dot(hidden, w_down[0], preferred_element_type=jnp.float32)
    reduced = sent_and_summed(partial_value.astype(jnp.bfloat16), "tp", 1).astype(jnp.bfloat16)
    returned = lax.all_to_all(
        reduced.reshape(ep_count, capacity, -1), EP, split_axis=0, concat_axis=0, tiled=True
    )
    quarter = returned.shape[2]
    summed = returned.reshape(experts, HALVES, capacity, quarter).astype(jnp.float32).sum(axis=1)
    picked = summed.reshape(experts * capacity, quarter)[place].reshape(
        tok_rows, top_count, quarter
    )
    mixed = jnp.sum(route_weight[:, :, None] * picked, axis=1)
    return mixed.astype(jnp.bfloat16)


def solution(mesh):
    finer = Mesh(mesh.devices.reshape(8, 4, 2, mesh.shape["tp"]), ("ep_0", "ep_1", "ep_2", "tp"))
    in_specs = (
        P(EP, None),
        P(),
        P(EP, None),
        P(EP, None),
        P(EP, None, "tp"),
        P(EP, None, "tp"),
        P(EP, "tp", None),
    )
    out_specs = P(EP, "tp")
    return jax.shard_map(body, mesh=finer, in_specs=in_specs, out_specs=out_specs, check_vma=False)
```

profile of v0, /device:TPU:1, one launch (start us, length us, event | category | flops | bytes accessed | tf_op | source)
XLA Modules:
  0.0 284.4 jit_solution(11001555768529312184)
XLA Ops:
  0.0 0.9 copy.27
  1.1 1.2 reduce-window.6
  2.6 0.7 broadcast_multiply_fusion
  3.9 2.4 scatter_custom_fusion
  6.4 1.4 convert_reduce_fusion.1
  7.9 1.6 fusion.6
  9.5 0.4 fusion.8
  10.0 4.1 %gather_fusion = bf16[640,2048]{1,0:T(8,128)(2,1)} fusion(bf16[257,2048]{1,0:T(8,128)(2,1)S(1)} %concatenate.6, s32[1024]{0:T(1024)S(1)} %pad_clamp_fusion.1), kind=kCustom, calls=%fused_computation | custom fusion | bytes 5245440 | tf_op jit(solution)/shard_map/gather | solution.py:78
  14.1 5.4 %reshape_reshape_reshape_reshape.3 = bf16[32,2,1,10,2048]{4,3,1,0,2:T(8,128)(2,1)} reshape(bf16[640,2048]{1,0:T(8,128)(2,1)} %gather_fusion) | data formatting | bytes 5242880 | tf_op jit(solution)/shard_map/reshape;reshape;reshape;reshape | solution.py:28
  19.5 4.9 %copy.31 = bf16[32,2,1,10,2048]{4,1,3,2,0:T(2,128)(2,1)S(1)} copy(bf16[32,2,1,10,2048]{4,3,1,0,2:T(8,128)(2,1)} %reshape_reshape_reshape_reshape.3) | data formatting | bytes 5242880 | tf_op jit(solution)/shard_map/reshape;reshape;reshape;reshape | solution.py:28
  24.4 72.9 %all_to_all.20 = bf16[32,2,1,10,2048]{4,1,3,2,0:T(2,128)(2,1)S(1)} all-to-all(bf16[32,2,1,10,2048]{4,1,3,2,0:T(2,128)(2,1)S(1)} %copy.31), channel_id=1, replica_groups=mesh['ep_0'=8,'ep_1'=4,'ep_2'=2,'tp'=4] {'ep_0','ep_1'}, dimensions={0} | all-to-all | bytes 5242880 | tf_op jit(solution)/shard_map/all_to_all | solution.py:30
  97.3 1.4 copy.32
  98.8 8.3 %all_to_all.21 = bf16[32,2,1,10,2048]{4,0,3,2,1:T(8,128)(2,1)S(1)} all-to-all(bf16[32,2,1,10,2048]{4,0,3,2,1:T(8,128)(2,1)S(1)} %copy.32), channel_id=1, replica_groups=mesh['ep_0'=8,'ep_1'=4,'ep_2'=2,'tp'=4] {'ep_2'}, dimensions={1} | all-to-all | bytes 5242880 | tf_op jit(solution)/shard_map/all_to_all | solution.py:30
  107.0 2.7 copy.33
  109.7 3.0 %reshape_reshape.3 = bf16[64,10,2048]{2,0,1:T(8,128)(2,1)} reshape(bf16[32,2,1,10,2048]{4,1,0,3,2:T(2,128)(2,1)S(1)} %copy.33) | data formatting | bytes 5242880 | tf_op jit(solution)/shard_map/reshape;reshape | solution.py:23
  112.7 0.3 collective-permute-start
  113.1 4.8 %collective-permute-done = bf16[64,10,2048]{2,0,1:T(8,128)(2,1)S(1)} collective-permute-done((bf16[64,10,2048]{2,0,1:T(8,128)(2,1)}, bf16[64,10,2048]{2,0,1:T(8,128)(2,1)S(1)}, u32[]{:S(2)}, u32[]{:S(2)}) %collective-permute-start) | collective-permute-done | bytes 2621472 | tf_op jit(solution)/shard_map/ppermute | solution.py:43
  117.9 2.1 broadcast_select_fusion.1
  120.0 0.5 pad_maximum_fusion
  120.4 5.6 %copy.34 = bf16[64,20,2048]{2,1,0:T(8,128)(2,1)} copy(bf16[64,20,2048]{2,0,1:T(8,128)(2,1)S(1)} %pad_maximum_fusion) | data formatting | bytes 10485760 | tf_op jit(solution)/shard_map/concatenate | solution.py:85
  126.0 9.0 %reshape.183 = bf16[1280,2048]{1,0:T(8,128)(2,1)} reshape(bf16[64,20,2048]{2,1,0:T(8,128)(2,1)} %copy.34) | data formatting | bytes 10485760 | tf_op jit(solution)/shard_map/reshape | solution.py:86
  135.0 10.0 %fusion.2 = f32[1280,896]{1,0:T(8,128)} fusion(bf16[1280,2048]{1,0:T(8,128)(2,1)} %reshape.183, bf16[1,2048,896]{2,1,0:T(8,128)(2,1)} %param.11), kind=kOutput, calls=%fused_computation.9 | convolution fusion | flops 4697620480 | bytes 13500416 | tf_op jit(solution)/shard_map/dot_general | solution.py:87
  145.0 17.6 %convolution_convert_fusion = bf16[1280,2048]{1,0:T(8,128)(2,1)} fusion(bf16[1,896,2048]{2,1,0:T(8,128)(2,1)} %param.13, f32[1280,896]{1,0:T(8,128)} %fusion.2, bf16[1280,2048]{1,0:T(8,128)(2,1)} %reshape.183, bf16[1,2048,896]{2,1,0:T(8,128)(2,1)} %param.12), kind=kOutput, calls=%fused_computation.3 | convolution fusion | flops 9404743680 | bytes 22413312 | tf_op jit(solution)/shard_map/dot_general | solution.py:90
  162.6 3.0 %copy.38 = bf16[160,4,8,512]{3,2,0,1:T(8,128)(2,1)S(1)} copy(bf16[160,4,8,512]{3,2,1,0:T(8,128)(2,1)} %bitcast.49) | data formatting | bytes 10485760 | tf_op jit(solution)/shard_map/reshape | solution.py:16
  165.6 63.2 %all_to_all.22 = bf16[4,1280,512]{2,1,0:T(8,128)(2,1)} all-to-all(bf16[4,1280,512]{2,1,0:T(8,128)(2,1)S(1)} %bitcast.48), channel_id=1, replica_groups=mesh['ep_0'=8,'ep_1'=4,'ep_2'=2,'tp'=4] {'tp'}, dimensions={0} | all-to-all | bytes 10485760 | tf_op jit(solution)/shard_map/all_to_all | solution.py:48
  228.7 4.2 %reduce_sum.63 = bf16[1280,512]{1,0:T(8,128)(2,1)S(1)} reduce(bf16[4,1280,512]{2,1,0:T(8,128)(2,1)} %all_to_all.22, bf16[]{:T(256)} %constant.65.clone.1), dimensions={0}, to_apply=%region_6.7 | reduce | flops 1966080 | bytes 6553602 | tf_op jit(solution)/shard_map/reduce_sum | solution.py:49
  232.9 1.3 reshape.185
  234.2 6.4 %all-to-all-start.3 = ((bf16[64,20,512]{2,1,0:T(8,128)(2,1)}), bf16[64,20,512]{2,1,0:T(8,128)(2,1)S(1)}, u32[]{:S(2)}, u32[]{:S(2)}) async-start(bf16[64,20,512]{2,1,0:T(8,128)(2,1)} %reshape.185), calls=%async_computation.3 | async-start | bytes 3145728 | tf_op jit(solution)/shard_map/all_to_all | solution.py:92
  240.8 38.9 %all-to-all-done.3 = bf16[64,20,512]{2,1,0:T(8,128)(2,1)S(1)} async-done(((bf16[64,20,512]{2,1,0:T(8,128)(2,1)}), bf16[64,20,512]{2,1,0:T(8,128)(2,1)S(1)}, u32[]{:S(2)}, u32[]{:S(2)}) %all-to-all-start.3) | async-done | bytes 1310752 | tf_op jit(solution)/shard_map/all_to_all | solution.py:92
  280.1 1.6 gather_fusion.1
  281.7 0.6 reshape.187
  282.4 2.1 multiply_reduce_fusion
  (29 shorter events, 1.8 us)
Async XLA Ops:
  0.0 9.5 %copy-start = (bf16[256,2048]{1,0:T(8,128)(2,1)S(1)}, bf16[256,2048]{1,0:T(8,128)(2,1)}, u32[]{:S(2)}) copy-start(bf16[256,2048]{1,0:T(8,128)(2,1)} %param.7) | copy-start | bytes 3145732
  0.0 9.5 %copy-start.1 = (f32[2048]{0:T(1024)S(1)}, f32[2048]{0:T(1024)}, u32[]{:S(2)}) copy-start(f32[2048]{0:T(1024)} %param.8) | copy-start | bytes 24580
  112.7 5.1 %collective-permute-start = (bf16[64,10,2048]{2,0,1:T(8,128)(2,1)}, bf16[64,10,2048]{2,0,1:T(8,128)(2,1)S(1)}, u32[]{:S(2)}, u32[]{:S(2)}) collective-permute-start(bf16[64,10,2048]{2,0,1:T(8,128)(2,1)} %reshape_reshape.3), channel_id=1, source_target_pairs={{0,4},{4,0},{8,12},{12,8},{16,20},{20,16},{24,28},{28,24},{32,36},... | collective-permute-start | bytes 7864328 | tf_op jit(solution)/shard_map/ppermute | solution.py:43
  232.9 7.7 %copy-start.2 = (f32[256,2]{0,1:T(2,128)S(1)}, f32[256,2]{0,1:T(2,128)}, u32[]{:S(2)}) copy-start(f32[256,2]{0,1:T(2,128)} %param.10) | copy-start | bytes 6148
  234.2 45.5 %all-to-all-start.3 = ((bf16[64,20,512]{2,1,0:T(8,128)(2,1)}), bf16[64,20,512]{2,1,0:T(8,128)(2,1)S(1)}, u32[]{:S(2)}, u32[]{:S(2)}) async-start(bf16[64,20,512]{2,1,0:T(8,128)(2,1)} %reshape.185), calls=%async_computation.3 | async-start | bytes 3145728 | tf_op jit(solution)/shard_map/all_to_all | solution.py:92
where the time goes:
time: 285 us; the launch traced here: 284 us
  blocking collectives  144 us (51%)
  local copies, waits for them, and re-layouts  47.3 us (17%)
  waiting for transfers between devices  43.7 us (15%)
  matrix products  27.5 us (10%)
  other arithmetic  14.6 us (5%)
  starting transfers between devices  6.7 us (2%)
    all_to_all x2, blocking collectives, exchange_in_order(): out = lax.all_to_all(out, axes[k], k, k, tiled=True)  81.2 us
    all_to_all x1, blocking collectives, sent_and_summed(): parts = lax.all_to_all(split_up(array, dim, count), axis, 0, 0, tiled=True)  63.2 us
    all_to_all x1, waiting for transfers between devices, body(): lax.all_to_all(reduced.reshape(ep_count, capacity, -1), EP, split_axis=0,...  38.9 us
    dot_general x1, matrix products, body(): jnp.dot(hidden, w_down[0], preferred_element_type=jnp.float32)  17.6 us
    another operation x2, local copies, waits for them, and re-layouts, exchange_in_order(): out = parts.reshape(*(lax.axis_size(a) for a in axes), *inside)  10.3 us
    dot_general x1, matrix products, body(): gate = jnp.dot(routed, w_gate[0], preferred_element_type=jnp.float32)  9.98 us
    reshape x1, local copies, waits for them, and re-layouts, body(): routed = arrived.reshape(-1, width)  9 us
    all_to_all x1, starting transfers between devices, body(): lax.all_to_all(reduced.reshape(ep_count, capacity, -1), EP, split_axis=0,...  6.39 us
  transfers between devices with their start and end apart: 2, of which 2 were waited for; matrix products, arithmetic and copies ran while one was open for 0% of the time, Pallas kernels for 0%

commit v1 on v0

v1 whole, which is shorter than its diff:
```python
import functools

import jax
import jax.numpy as jnp
from jax import lax
from jax.experimental import pallas as pl
from jax.experimental.pallas import tpu as pltpu
from jax.sharding import Mesh
from jax.sharding import PartitionSpec as P


EPSILON = 1e-05
EP = ("z", "y", "c")
CAP, MAIN, REST = 20, 16, 4
LANES = 128
NONE = -64.0
BF, F32 = jnp.bfloat16, jnp.float32
MIB = 1024 * 1024


dot = functools.partial(jnp.dot, preferred_element_type=F32)


def whole(space=pltpu.VMEM):
    return pl.BlockSpec(memory_space=space)


def iota(shape, dim):
    return lax.broadcasted_iota(jnp.int32, shape, dim)


def moved(groups, k, dtype=BF):
    plain = (REST * groups, MAIN * groups)
    group_of = iota(plain, 0) // REST == iota(plain, 1) // MAIN
    same = iota(plain, 1) % MAIN == iota(plain, 0) % REST + k * REST
    return jnp.where(group_of & same, 1.0, 0.0).astype(dtype)


def packed(main, rest, write):
    groups, parts = main.shape[0] // MAIN, main.shape[1] // LANES
    last = None
    for k in range(parts):
        here = slice(k * LANES, (k + 1) * LANES)
        write(slice(k * MAIN, (k + 1) * MAIN), main[:, here].reshape(groups, MAIN, LANES))
        term = lax.dot_general(moved(groups, k), rest[:, here], (((0,), (0,)), ((), ())), preferred_element_type=F32)
        last = term if last is None else last + term
    write(slice(parts * MAIN, parts * (MAIN + REST)), last.astype(BF).reshape(groups, MAIN, LANES))


def unpacked(read, groups, parts, write):
    last = read(slice(parts * MAIN, parts * (MAIN + REST))).reshape(groups * MAIN, LANES)
    for k in range(parts):
        here = slice(k * LANES, (k + 1) * LANES)
        write(slice(0, groups * MAIN), here, read(slice(k * MAIN, (k + 1) * MAIN)).reshape(groups * MAIN, LANES))
        write(slice(groups * MAIN, groups * CAP), here, dot(moved(groups, k), last).astype(BF))


def rows_of_experts(experts, flip):
    rows = experts * CAP
    row, expert = (iota((rows, experts), 0), iota((rows, experts), 1))
    first = experts * MAIN
    owner = jnp.where(row < first, row // MAIN, (row - first) // REST)
    spread = jnp.where(owner == expert, 1.0, 0.0).astype(BF)
    shape, dim = ((1, rows), 1) if flip else ((rows, 1), 0)
    at = iota(shape, dim)
    slot = jnp.where(at < first, at % MAIN, MAIN + (at - first) % REST).astype(F32)
    return spread, slot


def prep_kernel(sel, tokens, gain_hbm, ids_hbm, weight_hbm, message, slots, high, low, tok, gain, ids, weight, sems):
    copies = [
        pltpu.make_async_copy(source, target, sems.at[n])
        for n, (source, target) in enumerate(
            ((ids_hbm, ids), (tokens, tok), (gain_hbm, gain), (weight_hbm, weight))
        )
    ]
    for copy in copies:
        copy.start()
    rows, width = tok.shape
    experts = slots.shape[0]
    quarter = message.shape[1] // CAP * LANES
    copies[0].wait()
    number = iota((experts, rows), 0)
    first, second = number == ids[0:1, :], number == ids[1:2, :]
    named = jnp.where(first | second, 1.0, 0.0)
    earlier = jnp.where(iota((rows, rows), 0) < iota((rows, rows), 1), 1.0, 0.0).astype(BF)
    slot = jnp.where(named > 0, dot(named.astype(BF), earlier), NONE).astype(BF)
    slots[...] = slot
    spread, wanted = rows_of_experts(experts, False)
    pick = jnp.where(dot(spread, slot) == wanted, 1.0, 0.0).astype(BF)
    for copy in copies[1:]:
        copy.wait()
    scale = jnp.where(first, weight[0:1, :], 0.0) + jnp.where(second, weight[1:2, :], 0.0)
    high[...] = scale.astype(BF)
    low[...] = (scale - scale.astype(BF).astype(F32)).astype(BF)
    values = tok[...].astype(F32)
    mean = jnp.sum(values, axis=1, keepdims=True) * (1.0 / width)
    center = values - mean
    variance = jnp.sum(center * center, axis=1, keepdims=True) * (1.0 / width)
    columns = pl.ds(pl.multiple_of(sel[0] * quarter, quarter), quarter)
    part = tok[:, columns].astype(F32) - mean
    normed = (part * lax.rsqrt(variance + EPSILON) * gain[:, columns]).astype(BF)
    routed = dot(pick, normed).astype(BF)

    def write(at, value):
        message[:, at, :] = value

    packed(routed[: experts * MAIN], routed[experts * MAIN :], write)


def arrange_kernel(message, *outs):
    groups, parts = message.shape[0] // len(outs), message.shape[1] // CAP
    for number, out in enumerate(outs):
        here = slice(number * groups, (number + 1) * groups)

        def write(rows, columns, value):
            out[rows, columns] = value

        unpacked(lambda at: message[here, at, :], groups, parts, write)


def collect_kernel(*refs, count):
    message = refs[3 * count]
    groups = message.shape[0] // count
    for number in range(count):
        here = slice(number * groups, (number + 1) * groups)
        total = sum(r[...].astype(F32) for r in refs[3 * number : 3 * number + 3]).astype(BF)

        def write(at, value):
            message[here, at, :] = value

        packed(total[: groups * MAIN], total[groups * MAIN :], write)


def mixer_kernel(slots, high, low, mix_high, mix_low):
    spread, wanted = rows_of_experts(slots.shape[0], True)

    def of_rows(value):
        return lax.dot_general(value[...], spread, (((0,), (1,)), ((), ())), preferred_element_type=F32)

    named = of_rows(slots) == wanted
    for scale, mix in ((high, mix_high), (low, mix_low)):
        mix[...] = jnp.where(named, of_rows(scale), 0.0).astype(BF)


def combine_kernel(message, mix_high, mix_low, out, plain):
    def write(rows, columns, value):
        plain[rows, columns] = value

    unpacked(lambda at: message[:, at, :], message.shape[0], message.shape[1] // CAP, write)
    out[...] = (dot(mix_high[...], plain[...]) + dot(mix_low[...], plain[...])).astype(BF)


def stage_kernel(gate, up, down, both, out, sems):
    hidden = gate.shape[2]
    copies = [pltpu.make_async_copy(down.at[0], out, sems.at[0])]
    for j in range(hidden // LANES):
        for which, weight in ((0, gate), (1, up)):
            here = 2 * j + which
            copies.append(
                pltpu.make_async_copy(
                    weight.at[0, :, j * LANES : (j + 1) * LANES],
                    both.at[:, here * LANES : (here + 1) * LANES],
                    sems.at[1 + here],
                )
            )
    for copy in copies:
        copy.start()
    for copy in copies:
        copy.wait()


def expert_kernel(sel, *refs):
    pieces, (both_0, down_0, both_1, down_1), refs = refs[:4], refs[4:8], refs[8:]
    outs, (rows, hidden) = refs[:4], refs[4:]
    quarter = pieces[0].shape[1]
    width = down_0.shape[0]
    for k in range(4):
        rows[:, pl.ds(pl.multiple_of(sel[k] * quarter, quarter), quarter)] = pieces[k][...]
    for half, both in enumerate((both_0, both_1)):
        values = dot(rows[...], both[...])
        for j in range(width // LANES):
            gate = values[:, 2 * j * LANES : (2 * j + 1) * LANES]
            up = values[:, (2 * j + 1) * LANES : (2 * j + 2) * LANES]
            at = half * width + j * LANES
            hidden[:, at : at + LANES] = (gate / (1.0 + jnp.exp(-gate)) * up).astype(BF)
    for k in range(4):
        here = pl.ds(pl.multiple_of(sel[4 + k] * quarter, quarter), quarter)
        part = dot(hidden[:, :width], down_0[:, here]) + dot(hidden[:, width:], down_1[:, here])
        outs[k][...] = part.astype(BF)


def add_kernel(a, b, out):
    out[...] = (a[...].astype(F32) + b[...].astype(F32)).astype(BF)


def call(kernel, args, outs, scratch=(), spaces=None, limit=12, flops=1 << 28):
    spaces = spaces or [pltpu.VMEM] * len(args)
    args = [pltpu.with_memory_space_constraint(a, s) if s == pltpu.HBM else a for a, s in zip(args, spaces, strict=True)]
    return pl.pallas_call(
        kernel,
        in_specs=[whole(space) for space in spaces],
        out_specs=[whole()] * len(outs),
        out_shape=outs,
        scratch_shapes=scratch,
        compiler_params=pltpu.CompilerParams(vmem_limit_bytes=limit * MIB),
        cost_estimate=pl.CostEstimate(flops=flops, bytes_accessed=4 * MIB, transcendentals=0),
    )(*args)


def layer(tokens, norm_gain, expert_ids, route_weight, w_gate, w_up, w_down):
    tok_rows, width = tokens.shape
    experts = lax.axis_size("z") * lax.axis_size("y")
    across = lax.axis_size("x")
    quarter = width // across
    parts = quarter // LANES
    hidden = w_gate.shape[2]
    x = lax.axis_index("x")
    shape = jax.ShapeDtypeStruct
    dma = pltpu.SemaphoreType.DMA

    def shift(value, by):
        return lax.ppermute(value, "x", [(i, (i + by) % across) for i in range(across)])

    def exchange(value):
        return lax.all_to_all(value, ("z", "y"), 0, 0, tiled=True)

    near = [(x + by) % across for by in (0, 1, 3, 2)]
    sel = jnp.stack([near[k] for k in (0, 2, 1, 3, 0, 1, 2, 3)]).astype(jnp.int32)

    theirs = [lax.ppermute(w, "c", [(0, 1), (1, 0)]) for w in (w_gate, w_up, w_down)]
    message = shape((experts, parts * CAP, LANES), BF)
    table = shape((experts, tok_rows), BF)
    hbm = pltpu.HBM
    send, slots, high, low = call(
        prep_kernel,
        [sel, tokens, norm_gain.reshape(1, width), expert_ids.T, route_weight.T],
        [message, table, table, table],
        [
            pltpu.VMEM(tokens.shape, BF),
            pltpu.VMEM((1, width), F32),
            pltpu.VMEM(expert_ids.shape[::-1], jnp.int32),
            pltpu.VMEM(expert_ids.shape[::-1], F32),
            dma((4,)),
        ],
        spaces=[pltpu.SMEM, hbm, hbm, hbm, hbm],
    )
    arrived = exchange(send)
    weights = []
    for g, u, d in ((w_gate, w_up, w_down), theirs):
        weights += call(
            stage_kernel,
            [g, u, d],
            [pltpu.VMEM((width, 2 * hidden), BF), pltpu.VMEM((hidden, width), BF)],
            [dma((1 + 2 * hidden // LANES,))],
            spaces=[hbm] * 3,
            flops=1 << 31,
        )
    mix = shape((tok_rows, experts * CAP), BF)
    mixers = call(mixer_kernel, [slots, high, low], [mix, mix], flops=1 << 30)

    count = 2
    rows = experts * CAP // count
    piece = shape((rows, quarter), BF)
    chunks = call(arrange_kernel, [arrived], [piece] * count)
    sums = []
    for number, mine in enumerate(chunks):
        way = 1 if number % 2 == 0 else -1
        left = shift(mine, 1)
        right = shift(mine, -1)
        far = shift(left if way == 1 else right, way)
        outs = call(
            expert_kernel,
            [sel, mine, left, right, far, *weights],
            [piece] * 4,
            [pltpu.VMEM((rows, width), BF), pltpu.VMEM((rows, 2 * hidden), BF)],
            spaces=[pltpu.SMEM] + [pltpu.VMEM] * 8,
            limit=20,
            flops=12 * rows * width * hidden,
        )
        passed = shift(outs[3], way)
        near_by = 1 if way == 1 else 2
        direct = shift(outs[3 - near_by], -way)
        relay = call(add_kernel, [outs[near_by], passed], [piece])[0]
        sums += [outs[0], direct, shift(relay, way)]
    back = call(functools.partial(collect_kernel, count=count), sums, [message])[0]
    returned = exchange(back)
    return call(
        combine_kernel,
        [returned, *mixers],
        [shape((tok_rows, quarter), BF)],
        [pltpu.VMEM((experts * CAP, quarter), BF)],
    )[0]


def solution(mesh):
    finer = Mesh(mesh.devices.reshape(8, 4, 2, mesh.shape["tp"]), ("z", "y", "c", "x"))
    in_specs = (
        P(EP, None),
        P(),
        P(EP, None),
        P(EP, None),
        P(EP, None, "x"),
        P(EP, None, "x"),
        P(EP, "x", None),
    )
    return jax.shard_map(layer, mesh=finer, in_specs=in_specs, out_specs=P(EP, "x"), check_vma=False)
```

time: 285 us -> 127 us (0.45)
  the two profiles are of different devices: /device:TPU:1 before, /device:TPU:8 now
where the time goes in v1:
time: 127 us
  waiting for transfers between devices  40.6 us (32%)
  Pallas kernels  32.5 us (26%)
  blocking collectives  31.8 us (25%)
  starting transfers between devices  21.7 us (17%)
    pallas_call x11, Pallas kernels, call(): pl.pallas_call(kernel, in_specs=[whole(space) for space in spaces], out_s...  32.5 us
    all_to_all x1, blocking collectives, exchange(): return lax.all_to_all(value, ('z', 'y'), 0, 0, tiled=True)  31.8 us
    ppermute x12, waiting for transfers between devices, shift(): lax.ppermute(value, 'x', [(i, (i + by) % across) for i in range(across)])  24.8 us
    all_to_all x1, waiting for transfers between devices, exchange(): return lax.all_to_all(value, ('z', 'y'), 0, 0, tiled=True)  15.8 us
    ppermute x12, starting transfers between devices, shift(): lax.ppermute(value, 'x', [(i, (i + by) % across) for i in range(across)])  14.4 us
    all_to_all x1, starting transfers between devices, exchange(): return lax.all_to_all(value, ('z', 'y'), 0, 0, tiled=True)  6.75 us
  transfers between devices with their start and end apart: 16, of which 6 were waited for; matrix products, arithmetic and copies ran while one was open for 0% of the time, Pallas kernels for 23%

profile of v1, /device:TPU:8, one launch (start us, length us, event | category | flops | bytes accessed | tf_op | source)
XLA Modules:
  0.0 126.8 jit_solution(2099970707066135823)
XLA Ops:
  0.0 0.5 collective-permute-start.4
  0.5 0.0 collective-permute-start.5
  0.5 0.1 stack.23.sel
  0.6 3.0 %shard_map.73 = (bf16[32,80,128]{2,1,0:T(8,128)(2,1)S(1)}, bf16[32,256]{1,0:T(8,128)(2,1)S(1)}, bf16[32,256]{1,0:T(8,128)(2,1)S(1)}, bf16[32,256]{1,0:T(8,128)(2,1)S(1)}) custom-call(s32[8]{0:T(128)S(1)} %stack.23.sel, bf16[256,2048]{1,0:T(8,128)(2,1)} %tokens.1, f32[1,2048]{1,0:T(1,128)} %bitcast.7, s32[2,256]{1,0:T(2,128)} %bitcast.8, f32[2,256]{1,0:T(2,128)} %bitcast.9), custom_call_target="tpu_custom_call" | custom-call | flops 268435456 | bytes 4194304 | tf_op jit(solution)/shard_map/pallas_call | solution.py:200
  3.6 31.8 %all_to_all.10.message = bf16[32,80,128]{2,1,0:T(8,128)(2,1)S(1)} all-to-all(bf16[32,80,128]{2,1,0:T(8,128)(2,1)S(1)} %get-tuple-element.25), channel_id=1, replica_groups=mesh['z'=8,'y'=4,'c'=2,'x'=4] {'z','y'}, dimensions={0} | all-to-all | bytes 1310720 | tf_op jit(solution)/shard_map/all_to_all | solution.py:226
  35.4 0.3 shard_map.74
  35.7 2.8 %collective-permute-start.10 = (bf16[320,512]{1,0:T(8,128)(2,1)S(1)}, bf16[320,512]{1,0:T(8,128)(2,1)S(1)}, u32[]{:S(2)}, u32[]{:S(2)}) collective-permute-start(bf16[320,512]{1,0:T(8,128)(2,1)S(1)} %get-tuple-element.35.refs_0_), channel_id=1, source_target_pairs={{0,3},{1,0},{2,1},{3,2},{4,7},{5,4},{6,5},{7,6},{8,11},{9,8},{10,9... | collective-permute-start | bytes 983048 | tf_op jit(solution)/shard_map/ppermute | solution.py:223
  38.5 5.8 %collective-permute-done.10.refs_2_ = bf16[320,512]{1,0:T(8,128)(2,1)S(1)} collective-permute-done((bf16[320,512]{1,0:T(8,128)(2,1)S(1)}, bf16[320,512]{1,0:T(8,128)(2,1)S(1)}, u32[]{:S(2)}, u32[]{:S(2)}) %collective-permute-start.10) | collective-permute-done | bytes 327712 | tf_op jit(solution)/shard_map/ppermute | solution.py:223
  44.3 1.2 collective-permute-start.9
  45.5 3.2 %collective-permute-done.refs_1_ = bf16[320,512]{1,0:T(8,128)(2,1)S(1)} collective-permute-done((bf16[320,512]{1,0:T(8,128)(2,1)S(1)}, bf16[320,512]{1,0:T(8,128)(2,1)S(1)}, u32[]{:S(2)}, u32[]{:S(2)}) %collective-permute-start) | collective-permute-done | bytes 327712 | tf_op jit(solution)/shard_map/ppermute | solution.py:223
  48.8 4.5 %shard_map.75 = (bf16[2048,1792]{1,0:T(8,128)(2,1)S(1)}, bf16[896,2048]{1,0:T(8,128)(2,1)S(1)}) custom-call(bf16[1,2048,896]{2,1,0:T(8,128)(2,1)} %gate.1, bf16[1,2048,896]{2,1,0:T(8,128)(2,1)} %up.1, bf16[1,896,2048]{2,1,0:T(8,128)(2,1)} %down.1), custom_call_target="tpu_custom_call" | custom-call | flops 2147483648 | bytes 4194304 | tf_op jit(solution)/shard_map/pallas_call | solution.py:200
  53.3 1.3 %collective-permute-start.1 = (bf16[320,512]{1,0:T(8,128)(2,1)S(1)}, bf16[320,512]{1,0:T(8,128)(2,1)S(1)}, u32[]{:S(2)}, u32[]{:S(2)}) collective-permute-start(bf16[320,512]{1,0:T(8,128)(2,1)S(1)} %get-tuple-element.26.refs_0_), channel_id=1, source_target_pairs={{0,3},{1,0},{2,1},{3,2},{4,7},{5,4},{6,5},{7,6},{8,11},{9,8},{10,9... | collective-permute-start | bytes 983048 | tf_op jit(solution)/shard_map/ppermute | solution.py:223
  54.6 1.0 collective-permute-start.2
  55.6 4.5 %shard_map.76 = (bf16[2048,1792]{1,0:T(8,128)(2,1)S(1)}, bf16[896,2048]{1,0:T(8,128)(2,1)S(1)}) custom-call(bf16[1,2048,896]{2,1,0:T(8,128)(2,1)} %collective-permute-done.3.gate, bf16[1,2048,896]{2,1,0:T(8,128)(2,1)} %collective-permute-done.4.up, bf16[1,896,2048]{2,1,0:T(8,128)(2,1)} %collective-permute-done.5.down), custom_call_target="tpu_custom_call" | custom-call | flops 2147483648 | bytes 4194304 | tf_op jit(solution)/shard_map/pallas_call | solution.py:200
  60.1 8.4 %shard_map.79 = (bf16[320,512]{1,0:T(8,128)(2,1)S(1)}, bf16[320,512]{1,0:T(8,128)(2,1)S(1)}, bf16[320,512]{1,0:T(8,128)(2,1)S(1)}, bf16[320,512]{1,0:T(8,128)(2,1)S(1)}) custom-call(s32[8]{0:T(128)S(1)} %stack.23.sel, bf16[320,512]{1,0:T(8,128)(2,1)S(1)} %get-tuple-element.35.refs_0_, bf16[320,512]{1,0:T(8,128)(2,1)S(1)} %collective-permute-done.9.refs_1_, ...), custom_call_target="tpu_custom_call" | custom-call | flops 7046430720 | bytes 4194304 | tf_op jit(solution)/shard_map/pallas_call | solution.py:200
  68.6 2.3 %collective-permute-start.13 = (bf16[320,512]{1,0:T(8,128)(2,1)S(1)}, bf16[320,512]{1,0:T(8,128)(2,1)S(1)}, u32[]{:S(2)}, u32[]{:S(2)}) collective-permute-start(bf16[320,512]{1,0:T(8,128)(2,1)S(1)} %get-tuple-element.39), channel_id=1, source_target_pairs={{0,3},{1,0},{2,1},{3,2},{4,7},{5,4},{6,5},{7,6},{8,11},{9,8},{10,9... | collective-permute-start | bytes 983048 | tf_op jit(solution)/shard_map/ppermute | solution.py:223
  70.8 8.4 %shard_map.77 = (bf16[320,512]{1,0:T(8,128)(2,1)S(1)}, bf16[320,512]{1,0:T(8,128)(2,1)S(1)}, bf16[320,512]{1,0:T(8,128)(2,1)S(1)}, bf16[320,512]{1,0:T(8,128)(2,1)S(1)}) custom-call(s32[8]{0:T(128)S(1)} %stack.23.sel, bf16[320,512]{1,0:T(8,128)(2,1)S(1)} %get-tuple-element.26.refs_0_, bf16[320,512]{1,0:T(8,128)(2,1)S(1)} %collective-permute-done.refs_1_, ...), custom_call_target="tpu_custom_call" | custom-call | flops 7046430720 | bytes 4194304 | tf_op jit(solution)/shard_map/pallas_call | solution.py:200
  79.3 0.3 collective-permute-start.7
  79.6 1.6 %collective-permute-start.12 = (bf16[320,512]{1,0:T(8,128)(2,1)S(1)}, bf16[320,512]{1,0:T(8,128)(2,1)S(1)}, u32[]{:S(2)}, u32[]{:S(2)}) collective-permute-start(bf16[320,512]{1,0:T(8,128)(2,1)S(1)} %get-tuple-element.37), channel_id=1, source_target_pairs={{0,1},{1,2},{2,3},{3,0},{4,5},{5,6},{6,7},{7,4},{8,9},{9,10},{10,1... | collective-permute-start | bytes 983048 | tf_op jit(solution)/shard_map/ppermute | solution.py:223
  81.1 1.8 %collective-permute-start.6 = (bf16[320,512]{1,0:T(8,128)(2,1)S(1)}, bf16[320,512]{1,0:T(8,128)(2,1)S(1)}, u32[]{:S(2)}, u32[]{:S(2)}) collective-permute-start(bf16[320,512]{1,0:T(8,128)(2,1)S(1)} %get-tuple-element.32), channel_id=1, source_target_pairs={{0,3},{1,0},{2,1},{3,2},{4,7},{5,4},{6,5},{7,6},{8,11},{9,8},{10,9... | collective-permute-start | bytes 983048 | tf_op jit(solution)/shard_map/ppermute | solution.py:223
  82.9 0.1 shard_map.80
  83.0 2.0 %collective-permute-start.14 = (bf16[320,512]{1,0:T(8,128)(2,1)S(1)}, bf16[320,512]{1,0:T(8,128)(2,1)S(1)}, u32[]{:S(2)}, u32[]{:S(2)}) collective-permute-start(bf16[320,512]{1,0:T(8,128)(2,1)S(1)} %shard_map.80), channel_id=1, source_target_pairs={{0,3},{1,0},{2,1},{3,2},{4,7},{5,4},{6,5},{7,6},{8,11},{9,8},{10,9... | collective-permute-start | bytes 983048 | tf_op jit(solution)/shard_map/ppermute | solution.py:223
  85.0 6.4 %collective-permute-done.7.b = bf16[320,512]{1,0:T(8,128)(2,1)S(1)} collective-permute-done((bf16[320,512]{1,0:T(8,128)(2,1)S(1)}, bf16[320,512]{1,0:T(8,128)(2,1)S(1)}, u32[]{:S(2)}, u32[]{:S(2)}) %collective-permute-start.7) | collective-permute-done | bytes 327712 | tf_op jit(solution)/shard_map/ppermute | solution.py:223
  91.3 0.1 shard_map.78
  91.4 0.1 collective-permute-start.8
  91.5 5.8 %collective-permute-done.12.refs_4_ = bf16[320,512]{1,0:T(8,128)(2,1)S(1)} collective-permute-done((bf16[320,512]{1,0:T(8,128)(2,1)S(1)}, bf16[320,512]{1,0:T(8,128)(2,1)S(1)}, u32[]{:S(2)}, u32[]{:S(2)}) %collective-permute-start.12) | collective-permute-done | bytes 327712 | tf_op jit(solution)/shard_map/ppermute | solution.py:223
  97.3 3.5 %collective-permute-done.8.refs_2_ = bf16[320,512]{1,0:T(8,128)(2,1)S(1)} collective-permute-done((bf16[320,512]{1,0:T(8,128)(2,1)S(1)}, bf16[320,512]{1,0:T(8,128)(2,1)S(1)}, u32[]{:S(2)}, u32[]{:S(2)}) %collective-permute-start.8) | collective-permute-done | bytes 327712 | tf_op jit(solution)/shard_map/ppermute | solution.py:223
  100.8 1.4 %shard_map.81 = bf16[32,80,128]{2,1,0:T(8,128)(2,1)} custom-call(bf16[320,512]{1,0:T(8,128)(2,1)S(1)} %get-tuple-element.31.refs_0_, bf16[320,512]{1,0:T(8,128)(2,1)S(1)} %collective-permute-done.6.refs_1_, bf16[320,512]{1,0:T(8,128)(2,1)S(1)} %collective-permute-done.8.refs_2_, bf16[320,512]{1,0:T(8,128)(2,1)S(1)} %get-tuple-element.36.refs_3_, ...), custom_call_target="tpu_custom_call" | custom-call | flops 268435456 | bytes 4194304 | tf_op jit(solution)/shard_map/pallas_call | solution.py:200
  102.3 6.7 %all-to-all-start.1 = ((bf16[32,80,128]{2,1,0:T(8,128)(2,1)}), bf16[32,80,128]{2,1,0:T(8,128)(2,1)S(1)}, u32[]{:S(2)}, u32[]{:S(2)}) async-start(bf16[32,80,128]{2,1,0:T(8,128)(2,1)} %shard_map.81), calls=%async_computation.1 | async-start | bytes 1310720 | tf_op jit(solution)/shard_map/all_to_all | solution.py:226
  109.1 0.4 shard_map.82
  109.5 15.8 %all-to-all-done.1.message = bf16[32,80,128]{2,1,0:T(8,128)(2,1)S(1)} async-done(((bf16[32,80,128]{2,1,0:T(8,128)(2,1)}), bf16[32,80,128]{2,1,0:T(8,128)(2,1)S(1)}, u32[]{:S(2)}, u32[]{:S(2)}) %all-to-all-start.1) | async-done | bytes 655392 | tf_op jit(solution)/shard_map/all_to_all | solution.py:226
  125.3 1.4 %shard_map.83 = bf16[256,512]{1,0:T(8,128)(2,1)} custom-call(bf16[32,80,128]{2,1,0:T(8,128)(2,1)S(1)} %all-to-all-done.1.message, bf16[256,640]{1,0:T(8,128)(2,1)S(1)} %get-tuple-element.43.mix_high, bf16[256,640]{1,0:T(8,128)(2,1)S(1)} %get-tuple-element.44.mix_low), custom_call_target="tpu_custom_call" | custom-call | flops 268435456 | bytes 4194304 | tf_op jit(solution)/shard_map/pallas_call | solution.py:200
  (13 shorter events, 0.0 us)
Async XLA Ops:
  0.0 53.2 %collective-permute-start.3 = (bf16[1,2048,896]{2,1,0:T(8,128)(2,1)}, bf16[1,2048,896]{2,1,0:T(8,128)(2,1)}, u32[]{:S(2)}, u32[]{:S(2)}) collective-permute-start(bf16[1,2048,896]{2,1,0:T(8,128)(2,1)} %gate.1), channel_id=1, source_target_pairs={{0,4},{4,0},{1,5},{5,1},{2,6},{6,2},{3,7},{7,3},{8,12},{12,8},{9,1... | collective-permute-start | bytes 11010056 | tf_op jit(solution)/shard_map/ppermute | solution.py:231
  0.0 54.6 %collective-permute-start.4 = (bf16[1,2048,896]{2,1,0:T(8,128)(2,1)}, bf16[1,2048,896]{2,1,0:T(8,128)(2,1)}, u32[]{:S(2)}, u32[]{:S(2)}) collective-permute-start(bf16[1,2048,896]{2,1,0:T(8,128)(2,1)} %up.1), channel_id=1, source_target_pairs={{0,4},{4,0},{1,5},{5,1},{2,6},{6,2},{3,7},{7,3},{8,12},{12,8},{9,1... | collective-permute-start | bytes 11010056 | tf_op jit(solution)/shard_map/ppermute | solution.py:231
  0.5 55.1 %collective-permute-start.5 = (bf16[1,896,2048]{2,1,0:T(8,128)(2,1)}, bf16[1,896,2048]{2,1,0:T(8,128)(2,1)}, u32[]{:S(2)}, u32[]{:S(2)}) collective-permute-start(bf16[1,896,2048]{2,1,0:T(8,128)(2,1)} %down.1), channel_id=1, source_target_pairs={{0,4},{4,0},{1,5},{5,1},{2,6},{6,2},{3,7},{7,3},{8,12},{12,8},{9,1... | collective-permute-start | bytes 11010056 | tf_op jit(solution)/shard_map/ppermute | solution.py:231
  35.7 8.7 %collective-permute-start.10 = (bf16[320,512]{1,0:T(8,128)(2,1)S(1)}, bf16[320,512]{1,0:T(8,128)(2,1)S(1)}, u32[]{:S(2)}, u32[]{:S(2)}) collective-permute-start(bf16[320,512]{1,0:T(8,128)(2,1)S(1)} %get-tuple-element.35.refs_0_), channel_id=1, source_target_pairs={{0,3},{1,0},{2,1},{3,2},{4,7},{5,4},{6,5},{7,6},{8,11},{9,8},{10,9... | collective-permute-start | bytes 983048 | tf_op jit(solution)/shard_map/ppermute | solution.py:223
  38.5 10.3 %collective-permute-start = (bf16[320,512]{1,0:T(8,128)(2,1)S(1)}, bf16[320,512]{1,0:T(8,128)(2,1)S(1)}, u32[]{:S(2)}, u32[]{:S(2)}) collective-permute-start(bf16[320,512]{1,0:T(8,128)(2,1)S(1)} %get-tuple-element.26.refs_0_), channel_id=1, source_target_pairs={{0,1},{1,2},{2,3},{3,0},{4,5},{5,6},{6,7},{7,4},{8,9},{9,10},{10,1... | collective-permute-start | bytes 983048 | tf_op jit(solution)/shard_map/ppermute | solution.py:223
  44.3 15.8 %collective-permute-start.9 = (bf16[320,512]{1,0:T(8,128)(2,1)S(1)}, bf16[320,512]{1,0:T(8,128)(2,1)S(1)}, u32[]{:S(2)}, u32[]{:S(2)}) collective-permute-start(bf16[320,512]{1,0:T(8,128)(2,1)S(1)} %get-tuple-element.35.refs_0_), channel_id=1, source_target_pairs={{0,1},{1,2},{2,3},{3,0},{4,5},{5,6},{6,7},{7,4},{8,9},{9,10},{10,1... | collective-permute-start | bytes 983048 | tf_op jit(solution)/shard_map/ppermute | solution.py:223
  48.8 11.4 %collective-permute-start.11 = (bf16[320,512]{1,0:T(8,128)(2,1)S(1)}, bf16[320,512]{1,0:T(8,128)(2,1)S(1)}, u32[]{:S(2)}, u32[]{:S(2)}) collective-permute-start(bf16[320,512]{1,0:T(8,128)(2,1)S(1)} %collective-permute-done.10.refs_2_), channel_id=1, source_target_pairs={{0,3},{1,0},{2,1},{3,2},{4,7},{5,4},{6,5},{7,6},{8,11},{9,8},{10,9... | collective-permute-start | bytes 983048 | tf_op jit(solution)/shard_map/ppermute | solution.py:223
  53.3 17.6 %collective-permute-start.1 = (bf16[320,512]{1,0:T(8,128)(2,1)S(1)}, bf16[320,512]{1,0:T(8,128)(2,1)S(1)}, u32[]{:S(2)}, u32[]{:S(2)}) collective-permute-start(bf16[320,512]{1,0:T(8,128)(2,1)S(1)} %get-tuple-element.26.refs_0_), channel_id=1, source_target_pairs={{0,3},{1,0},{2,1},{3,2},{4,7},{5,4},{6,5},{7,6},{8,11},{9,8},{10,9... | collective-permute-start | bytes 983048 | tf_op jit(solution)/shard_map/ppermute | solution.py:223
  54.6 16.2 %collective-permute-start.2 = (bf16[320,512]{1,0:T(8,128)(2,1)S(1)}, bf16[320,512]{1,0:T(8,128)(2,1)S(1)}, u32[]{:S(2)}, u32[]{:S(2)}) collective-permute-start(bf16[320,512]{1,0:T(8,128)(2,1)S(1)} %collective-permute-done.refs_1_), channel_id=1, source_target_pairs={{0,1},{1,2},{2,3},{3,0},{4,5},{5,6},{6,7},{7,4},{8,9},{9,10},{10,1... | collective-permute-start | bytes 983048 | tf_op jit(solution)/shard_map/ppermute | solution.py:223
  68.6 14.3 %collective-permute-start.13 = (bf16[320,512]{1,0:T(8,128)(2,1)S(1)}, bf16[320,512]{1,0:T(8,128)(2,1)S(1)}, u32[]{:S(2)}, u32[]{:S(2)}) collective-permute-start(bf16[320,512]{1,0:T(8,128)(2,1)S(1)} %get-tuple-element.39), channel_id=1, source_target_pairs={{0,3},{1,0},{2,1},{3,2},{4,7},{5,4},{6,5},{7,6},{8,11},{9,8},{10,9... | collective-permute-start | bytes 983048 | tf_op jit(solution)/shard_map/ppermute | solution.py:223
  79.3 12.1 %collective-permute-start.7 = (bf16[320,512]{1,0:T(8,128)(2,1)S(1)}, bf16[320,512]{1,0:T(8,128)(2,1)S(1)}, u32[]{:S(2)}, u32[]{:S(2)}) collective-permute-start(bf16[320,512]{1,0:T(8,128)(2,1)S(1)} %get-tuple-element.34), channel_id=1, source_target_pairs={{0,1},{1,2},{2,3},{3,0},{4,5},{5,6},{6,7},{7,4},{8,9},{9,10},{10,1... | collective-permute-start | bytes 983048 | tf_op jit(solution)/shard_map/ppermute | solution.py:223
  79.6 17.8 %collective-permute-start.12 = (bf16[320,512]{1,0:T(8,128)(2,1)S(1)}, bf16[320,512]{1,0:T(8,128)(2,1)S(1)}, u32[]{:S(2)}, u32[]{:S(2)}) collective-permute-start(bf16[320,512]{1,0:T(8,128)(2,1)S(1)} %get-tuple-element.37), channel_id=1, source_target_pairs={{0,1},{1,2},{2,3},{3,0},{4,5},{5,6},{6,7},{7,4},{8,9},{9,10},{10,1... | collective-permute-start | bytes 983048 | tf_op jit(solution)/shard_map/ppermute | solution.py:223
  81.1 16.2 %collective-permute-start.6 = (bf16[320,512]{1,0:T(8,128)(2,1)S(1)}, bf16[320,512]{1,0:T(8,128)(2,1)S(1)}, u32[]{:S(2)}, u32[]{:S(2)}) collective-permute-start(bf16[320,512]{1,0:T(8,128)(2,1)S(1)} %get-tuple-element.32), channel_id=1, source_target_pairs={{0,3},{1,0},{2,1},{3,2},{4,7},{5,4},{6,5},{7,6},{8,11},{9,8},{10,9... | collective-permute-start | bytes 983048 | tf_op jit(solution)/shard_map/ppermute | solution.py:223
  83.0 14.4 %collective-permute-start.14 = (bf16[320,512]{1,0:T(8,128)(2,1)S(1)}, bf16[320,512]{1,0:T(8,128)(2,1)S(1)}, u32[]{:S(2)}, u32[]{:S(2)}) collective-permute-start(bf16[320,512]{1,0:T(8,128)(2,1)S(1)} %shard_map.80), channel_id=1, source_target_pairs={{0,3},{1,0},{2,1},{3,2},{4,7},{5,4},{6,5},{7,6},{8,11},{9,8},{10,9... | collective-permute-start | bytes 983048 | tf_op jit(solution)/shard_map/ppermute | solution.py:223
  91.4 9.4 %collective-permute-start.8 = (bf16[320,512]{1,0:T(8,128)(2,1)S(1)}, bf16[320,512]{1,0:T(8,128)(2,1)S(1)}, u32[]{:S(2)}, u32[]{:S(2)}) collective-permute-start(bf16[320,512]{1,0:T(8,128)(2,1)S(1)} %shard_map.78), channel_id=1, source_target_pairs={{0,1},{1,2},{2,3},{3,0},{4,5},{5,6},{6,7},{7,4},{8,9},{9,10},{10,1... | collective-permute-start | bytes 983048 | tf_op jit(solution)/shard_map/ppermute | solution.py:223
  102.3 23.0 %all-to-all-start.1 = ((bf16[32,80,128]{2,1,0:T(8,128)(2,1)}), bf16[32,80,128]{2,1,0:T(8,128)(2,1)S(1)}, u32[]{:S(2)}, u32[]{:S(2)}) async-start(bf16[32,80,128]{2,1,0:T(8,128)(2,1)} %shard_map.81), calls=%async_computation.1 | async-start | bytes 1310720 | tf_op jit(solution)/shard_map/all_to_all | solution.py:226

commit v2 on v1

--- a/solution.py
+++ b/solution.py
@@ -119,12 +119,13 @@
         unpacked(lambda at: message[here, at, :], groups, parts, write)
 
 
-def collect_kernel(*refs, count):
-    message = refs[3 * count]
-    groups = message.shape[0] // count
-    for number in range(count):
+def collect_kernel(own_0, own_1, relayed_0, direct_1, both, message):
+    groups = message.shape[0] // 2
+    rows = own_0.shape[0]
+    terms = (own_0, relayed_0, both.at[rows:, :]), (own_1, direct_1, both.at[:rows, :])
+    for number in range(2):
         here = slice(number * groups, (number + 1) * groups)
-        total = sum(r[...].astype(F32) for r in refs[3 * number : 3 * number + 3]).astype(BF)
+        total = sum(r[...].astype(F32) for r in terms[number]).astype(BF)
 
         def write(at, value):
             message[here, at, :] = value
@@ -190,8 +191,12 @@
         outs[k][...] = part.astype(BF)
 
 
-def add_kernel(a, b, out):
-    out[...] = (a[...].astype(F32) + b[...].astype(F32)).astype(BF)
+def add_kernel(a, b, *rest):
+    *behind, out = rest
+    rows = a.shape[0]
+    out[:rows, :] = (a[...].astype(F32) + b[...].astype(F32)).astype(BF)
+    for number, value in enumerate(behind):
+        out[(number + 1) * rows : (number + 2) * rows, :] = value[...]
 
 
 def call(kernel, args, outs, scratch=(), spaces=None, limit=12, flops=1 << 28):
@@ -263,27 +268,30 @@
     rows = experts * CAP // count
     piece = shape((rows, quarter), BF)
     chunks = call(arrange_kernel, [arrived], [piece] * count)
-    sums = []
-    for number, mine in enumerate(chunks):
-        way = 1 if number % 2 == 0 else -1
-        left = shift(mine, 1)
-        right = shift(mine, -1)
-        far = shift(left if way == 1 else right, way)
-        outs = call(
+    left_0, left_1 = (shift(chunks[n], 1) for n in range(count))
+    right_0, right_1 = (shift(chunks[n], -1) for n in range(count))
+    far_0, far_1 = shift(left_0, 1), shift(right_1, -1)
+
+    def expert(*pieces):
+        return call(
             expert_kernel,
-            [sel, mine, left, right, far, *weights],
+            [sel, *pieces, *weights],
             [piece] * 4,
             [pltpu.VMEM((rows, width), BF), pltpu.VMEM((rows, 2 * hidden), BF)],
             spaces=[pltpu.SMEM] + [pltpu.VMEM] * 8,
             limit=20,
             flops=12 * rows * width * hidden,
         )
-        passed = shift(outs[3], way)
-        near_by = 1 if way == 1 else 2
-        direct = shift(outs[3 - near_by], -way)
-        relay = call(add_kernel, [outs[near_by], passed], [piece])[0]
-        sums += [outs[0], direct, shift(relay, way)]
-    back = call(functools.partial(collect_kernel, count=count), sums, [message])[0]
+
+    own_1, next_1, last_1, far_1 = expert(chunks[1], left_1, right_1, far_1)
+    passed_1 = shift(far_1, -1)
+    direct_1 = shift(next_1, 1)
+    own_0, next_0, last_0, far_0 = expert(chunks[0], left_0, right_0, far_0)
+    passed_0 = shift(far_0, 1)
+    twice = shape((2 * rows, quarter), BF)
+    both = shift(call(add_kernel, [last_1, passed_1, last_0], [twice])[0], -1)
+    relayed_0 = shift(call(add_kernel, [next_0, passed_0], [piece])[0], 1)
+    back = call(collect_kernel, [own_0, own_1, relayed_0, direct_1, both], [message])[0]
     returned = exchange(back)
     return call(
         combine_kernel,

time: 127 us -> 127 us (level)
  starting transfers between devices: 21.7 us -> 19.6 us
  waiting for transfers between devices: 40.6 us -> 42.6 us
    ppermute x12 -> x11, starting transfers between devices: 14.4 us -> 12.4 us  [shift(): lax.ppermute(value, 'x', [(i, (i + by) % across) for i in range(across)])]
    ppermute x12 -> x11, waiting for transfers between devices: 24.8 us -> 26.8 us  [shift(): lax.ppermute(value, 'x', [(i, (i + by) % across) for i in range(across)])]
  transfers between devices with their start and end apart: 16 -> 15, of which waited for: 6 -> 6; matrix products, arithmetic and copies ran while one was open for 0% -> 0% of each run, Pallas kernels for 23% -> 23%
where the time goes in v2:
time: 127 us
  waiting for transfers between devices  42.6 us (34%)
  Pallas kernels  32.5 us (26%)
  blocking collectives  31.8 us (25%)
  starting transfers between devices  19.6 us (15%)
    pallas_call x11, Pallas kernels, call(): pl.pallas_call(kernel, in_specs=[whole(space) for space in spaces], out_s...  32.5 us
    all_to_all x1, blocking collectives, exchange(): return lax.all_to_all(value, ('z', 'y'), 0, 0, tiled=True)  31.8 us
    ppermute x11, waiting for transfers between devices, shift(): lax.ppermute(value, 'x', [(i, (i + by) % across) for i in range(across)])  26.8 us
    all_to_all x1, waiting for transfers between devices, exchange(): return lax.all_to_all(value, ('z', 'y'), 0, 0, tiled=True)  15.8 us
    ppermute x11, starting transfers between devices, shift(): lax.ppermute(value, 'x', [(i, (i + by) % across) for i in range(across)])  12.4 us
    all_to_all x1, starting transfers between devices, exchange(): return lax.all_to_all(value, ('z', 'y'), 0, 0, tiled=True)  6.75 us
  transfers between devices with their start and end apart: 15, of which 6 were waited for; matrix products, arithmetic and copies ran while one was open for 0% of the time, Pallas kernels for 23%

profile of v2, /device:TPU:8, one launch (start us, length us, event | category | flops | bytes accessed | tf_op | source)
XLA Modules:
  0.0 126.8 jit_solution(10591013499916746573)
XLA Ops:
  0.0 0.5 collective-permute-start.4
  0.5 0.0 collective-permute-start.5
  0.5 0.1 stack.23.sel
  0.6 3.0 %shard_map.73 = (bf16[32,80,128]{2,1,0:T(8,128)(2,1)S(1)}, bf16[32,256]{1,0:T(8,128)(2,1)S(1)}, bf16[32,256]{1,0:T(8,128)(2,1)S(1)}, bf16[32,256]{1,0:T(8,128)(2,1)S(1)}) custom-call(s32[8]{0:T(128)S(1)} %stack.23.sel, bf16[256,2048]{1,0:T(8,128)(2,1)} %tokens.1, f32[1,2048]{1,0:T(1,128)} %bitcast.7, s32[2,256]{1,0:T(2,128)} %bitcast.8, f32[2,256]{1,0:T(2,128)} %bitcast.9), custom_call_target="tpu_custom_call" | custom-call | flops 268435456 | bytes 4194304 | tf_op jit(solution)/shard_map/pallas_call | solution.py:205
  3.6 31.8 %all_to_all.10.message = bf16[32,80,128]{2,1,0:T(8,128)(2,1)S(1)} all-to-all(bf16[32,80,128]{2,1,0:T(8,128)(2,1)S(1)} %get-tuple-element.25), channel_id=1, replica_groups=mesh['z'=8,'y'=4,'c'=2,'x'=4] {'z','y'}, dimensions={0} | all-to-all | bytes 1310720 | tf_op jit(solution)/shard_map/all_to_all | solution.py:231
  35.4 0.3 shard_map.74
  35.7 2.8 %collective-permute-start.7 = (bf16[320,512]{1,0:T(8,128)(2,1)S(1)}, bf16[320,512]{1,0:T(8,128)(2,1)S(1)}, u32[]{:S(2)}, u32[]{:S(2)}) collective-permute-start(bf16[320,512]{1,0:T(8,128)(2,1)S(1)} %get-tuple-element.32.refs_0_), channel_id=1, source_target_pairs={{0,3},{1,0},{2,1},{3,2},{4,7},{5,4},{6,5},{7,6},{8,11},{9,8},{10,9... | collective-permute-start | bytes 983048 | tf_op jit(solution)/shard_map/ppermute | solution.py:228
  38.5 5.8 %collective-permute-done.7.refs_2_ = bf16[320,512]{1,0:T(8,128)(2,1)S(1)} collective-permute-done((bf16[320,512]{1,0:T(8,128)(2,1)S(1)}, bf16[320,512]{1,0:T(8,128)(2,1)S(1)}, u32[]{:S(2)}, u32[]{:S(2)}) %collective-permute-start.7) | collective-permute-done | bytes 327712 | tf_op jit(solution)/shard_map/ppermute | solution.py:228
  44.3 1.2 collective-permute-start.6
  45.5 3.2 %collective-permute-done.refs_1_ = bf16[320,512]{1,0:T(8,128)(2,1)S(1)} collective-permute-done((bf16[320,512]{1,0:T(8,128)(2,1)S(1)}, bf16[320,512]{1,0:T(8,128)(2,1)S(1)}, u32[]{:S(2)}, u32[]{:S(2)}) %collective-permute-start) | collective-permute-done | bytes 327712 | tf_op jit(solution)/shard_map/ppermute | solution.py:228
  48.8 0.0 collective-permute-start.8
  48.8 4.5 %shard_map.75 = (bf16[2048,1792]{1,0:T(8,128)(2,1)S(1)}, bf16[896,2048]{1,0:T(8,128)(2,1)S(1)}) custom-call(bf16[1,2048,896]{2,1,0:T(8,128)(2,1)} %gate.1, bf16[1,2048,896]{2,1,0:T(8,128)(2,1)} %up.1, bf16[1,896,2048]{2,1,0:T(8,128)(2,1)} %down.1), custom_call_target="tpu_custom_call" | custom-call | flops 2147483648 | bytes 4194304 | tf_op jit(solution)/shard_map/pallas_call | solution.py:205
  53.2 0.0 collective-permute-done.3.gate
  53.3 1.3 %collective-permute-start.1 = (bf16[320,512]{1,0:T(8,128)(2,1)S(1)}, bf16[320,512]{1,0:T(8,128)(2,1)S(1)}, u32[]{:S(2)}, u32[]{:S(2)}) collective-permute-start(bf16[320,512]{1,0:T(8,128)(2,1)S(1)} %get-tuple-element.26.refs_0_), channel_id=1, source_target_pairs={{0,3},{1,0},{2,1},{3,2},{4,7},{5,4},{6,5},{7,6},{8,11},{9,8},{10,9... | collective-permute-start | bytes 983048 | tf_op jit(solution)/shard_map/ppermute | solution.py:228
  54.6 1.0 collective-permute-start.2
  55.6 4.5 %shard_map.76 = (bf16[2048,1792]{1,0:T(8,128)(2,1)S(1)}, bf16[896,2048]{1,0:T(8,128)(2,1)S(1)}) custom-call(bf16[1,2048,896]{2,1,0:T(8,128)(2,1)} %collective-permute-done.3.gate, bf16[1,2048,896]{2,1,0:T(8,128)(2,1)} %collective-permute-done.4.up, bf16[1,896,2048]{2,1,0:T(8,128)(2,1)} %collective-permute-done.5.down), custom_call_target="tpu_custom_call" | custom-call | flops 2147483648 | bytes 4194304 | tf_op jit(solution)/shard_map/pallas_call | solution.py:205
  60.1 8.4 %shard_map.78 = (bf16[320,512]{1,0:T(8,128)(2,1)S(1)}, bf16[320,512]{1,0:T(8,128)(2,1)S(1)}, bf16[320,512]{1,0:T(8,128)(2,1)S(1)}, bf16[320,512]{1,0:T(8,128)(2,1)S(1)}) custom-call(s32[8]{0:T(128)S(1)} %stack.23.sel, bf16[320,512]{1,0:T(8,128)(2,1)S(1)} %get-tuple-element.32.refs_0_, bf16[320,512]{1,0:T(8,128)(2,1)S(1)} %collective-permute-done.6.refs_1_, ...), custom_call_target="tpu_custom_call" | custom-call | flops 7046430720 | bytes 4194304 | tf_op jit(solution)/shard_map/pallas_call | solution.py:205
  68.6 2.3 %collective-permute-start.12 = (bf16[320,512]{1,0:T(8,128)(2,1)S(1)}, bf16[320,512]{1,0:T(8,128)(2,1)S(1)}, u32[]{:S(2)}, u32[]{:S(2)}) collective-permute-start(bf16[320,512]{1,0:T(8,128)(2,1)S(1)} %get-tuple-element.38), channel_id=1, source_target_pairs={{0,3},{1,0},{2,1},{3,2},{4,7},{5,4},{6,5},{7,6},{8,11},{9,8},{10,9... | collective-permute-start | bytes 983048 | tf_op jit(solution)/shard_map/ppermute | solution.py:228
  70.8 8.4 %shard_map.77 = (bf16[320,512]{1,0:T(8,128)(2,1)S(1)}, bf16[320,512]{1,0:T(8,128)(2,1)S(1)}, bf16[320,512]{1,0:T(8,128)(2,1)S(1)}, bf16[320,512]{1,0:T(8,128)(2,1)S(1)}) custom-call(s32[8]{0:T(128)S(1)} %stack.23.sel, bf16[320,512]{1,0:T(8,128)(2,1)S(1)} %get-tuple-element.26.refs_0_, bf16[320,512]{1,0:T(8,128)(2,1)S(1)} %collective-permute-done.refs_1_, ...), custom_call_target="tpu_custom_call" | custom-call | flops 7046430720 | bytes 4194304 | tf_op jit(solution)/shard_map/pallas_call | solution.py:205
  79.3 0.3 collective-permute-start.9
  79.6 0.1 shard_map.80
  79.7 3.3 %collective-permute-start.13 = (bf16[640,512]{1,0:T(8,128)(2,1)S(1)}, bf16[640,512]{1,0:T(8,128)(2,1)S(1)}, u32[]{:S(2)}, u32[]{:S(2)}) collective-permute-start(bf16[640,512]{1,0:T(8,128)(2,1)S(1)} %shard_map.80), channel_id=1, source_target_pairs={{0,3},{1,0},{2,1},{3,2},{4,7},{5,4},{6,5},{7,6},{8,11},{9,8},{10,9... | collective-permute-start | bytes 1966088 | tf_op jit(solution)/shard_map/ppermute | solution.py:228
  83.0 8.4 %collective-permute-done.9.b = bf16[320,512]{1,0:T(8,128)(2,1)S(1)} collective-permute-done((bf16[320,512]{1,0:T(8,128)(2,1)S(1)}, bf16[320,512]{1,0:T(8,128)(2,1)S(1)}, u32[]{:S(2)}, u32[]{:S(2)}) %collective-permute-start.9) | collective-permute-done | bytes 327712 | tf_op jit(solution)/shard_map/ppermute | solution.py:228
  91.3 0.1 shard_map.79
  91.4 0.1 collective-permute-start.10
  91.5 5.8 %collective-permute-done.11.direct_1 = bf16[320,512]{1,0:T(8,128)(2,1)S(1)} collective-permute-done((bf16[320,512]{1,0:T(8,128)(2,1)S(1)}, bf16[320,512]{1,0:T(8,128)(2,1)S(1)}, u32[]{:S(2)}, u32[]{:S(2)}) %collective-permute-start.11) | collective-permute-done | bytes 327712 | tf_op jit(solution)/shard_map/ppermute | solution.py:228
  97.3 3.5 %collective-permute-done.10.relayed_0 = bf16[320,512]{1,0:T(8,128)(2,1)S(1)} collective-permute-done((bf16[320,512]{1,0:T(8,128)(2,1)S(1)}, bf16[320,512]{1,0:T(8,128)(2,1)S(1)}, u32[]{:S(2)}, u32[]{:S(2)}) %collective-permute-start.10) | collective-permute-done | bytes 327712 | tf_op jit(solution)/shard_map/ppermute | solution.py:228
  100.9 1.5 %shard_map.81 = bf16[32,80,128]{2,1,0:T(8,128)(2,1)} custom-call(bf16[320,512]{1,0:T(8,128)(2,1)S(1)} %get-tuple-element.31.own_0, bf16[320,512]{1,0:T(8,128)(2,1)S(1)} %get-tuple-element.33.own_1, bf16[320,512]{1,0:T(8,128)(2,1)S(1)} %collective-permute-done.10.relayed_0, bf16[320,512]{1,0:T(8,128)(2,1)S(1)} %collective-permute-done.11.direct_1, ...), custom_call_target="tpu_custom_call" | custom-call | flops 268435456 | bytes 4194304 | tf_op jit(solution)/shard_map/pallas_call | solution.py:205
  102.3 6.8 %all-to-all-start.1 = ((bf16[32,80,128]{2,1,0:T(8,128)(2,1)}), bf16[32,80,128]{2,1,0:T(8,128)(2,1)S(1)}, u32[]{:S(2)}, u32[]{:S(2)}) async-start(bf16[32,80,128]{2,1,0:T(8,128)(2,1)} %shard_map.81), calls=%async_computation.1 | async-start | bytes 1310720 | tf_op jit(solution)/shard_map/all_to_all | solution.py:231
  109.1 0.4 shard_map.82
  109.5 15.8 %all-to-all-done.1.message = bf16[32,80,128]{2,1,0:T(8,128)(2,1)S(1)} async-done(((bf16[32,80,128]{2,1,0:T(8,128)(2,1)}), bf16[32,80,128]{2,1,0:T(8,128)(2,1)S(1)}, u32[]{:S(2)}, u32[]{:S(2)}) %all-to-all-start.1) | async-done | bytes 655392 | tf_op jit(solution)/shard_map/all_to_all | solution.py:231
  125.3 1.4 %shard_map.83 = bf16[256,512]{1,0:T(8,128)(2,1)} custom-call(bf16[32,80,128]{2,1,0:T(8,128)(2,1)S(1)} %all-to-all-done.1.message, bf16[256,640]{1,0:T(8,128)(2,1)S(1)} %get-tuple-element.43.mix_high, bf16[256,640]{1,0:T(8,128)(2,1)S(1)} %get-tuple-element.44.mix_low), custom_call_target="tpu_custom_call" | custom-call | flops 268435456 | bytes 4194304 | tf_op jit(solution)/shard_map/pallas_call | solution.py:205
  (11 shorter events, 0.0 us)
Async XLA Ops:
  0.0 53.2 %collective-permute-start.3 = (bf16[1,2048,896]{2,1,0:T(8,128)(2,1)}, bf16[1,2048,896]{2,1,0:T(8,128)(2,1)}, u32[]{:S(2)}, u32[]{:S(2)}) collective-permute-start(bf16[1,2048,896]{2,1,0:T(8,128)(2,1)} %gate.1), channel_id=1, source_target_pairs={{0,4},{4,0},{1,5},{5,1},{2,6},{6,2},{3,7},{7,3},{8,12},{12,8},{9,1... | collective-permute-start | bytes 11010056 | tf_op jit(solution)/shard_map/ppermute | solution.py:236
  0.0 54.6 %collective-permute-start.4 = (bf16[1,2048,896]{2,1,0:T(8,128)(2,1)}, bf16[1,2048,896]{2,1,0:T(8,128)(2,1)}, u32[]{:S(2)}, u32[]{:S(2)}) collective-permute-start(bf16[1,2048,896]{2,1,0:T(8,128)(2,1)} %up.1), channel_id=1, source_target_pairs={{0,4},{4,0},{1,5},{5,1},{2,6},{6,2},{3,7},{7,3},{8,12},{12,8},{9,1... | collective-permute-start | bytes 11010056 | tf_op jit(solution)/shard_map/ppermute | solution.py:236
  0.5 55.1 %collective-permute-start.5 = (bf16[1,896,2048]{2,1,0:T(8,128)(2,1)}, bf16[1,896,2048]{2,1,0:T(8,128)(2,1)}, u32[]{:S(2)}, u32[]{:S(2)}) collective-permute-start(bf16[1,896,2048]{2,1,0:T(8,128)(2,1)} %down.1), channel_id=1, source_target_pairs={{0,4},{4,0},{1,5},{5,1},{2,6},{6,2},{3,7},{7,3},{8,12},{12,8},{9,1... | collective-permute-start | bytes 11010056 | tf_op jit(solution)/shard_map/ppermute | solution.py:236
  35.7 8.7 %collective-permute-start.7 = (bf16[320,512]{1,0:T(8,128)(2,1)S(1)}, bf16[320,512]{1,0:T(8,128)(2,1)S(1)}, u32[]{:S(2)}, u32[]{:S(2)}) collective-permute-start(bf16[320,512]{1,0:T(8,128)(2,1)S(1)} %get-tuple-element.32.refs_0_), channel_id=1, source_target_pairs={{0,3},{1,0},{2,1},{3,2},{4,7},{5,4},{6,5},{7,6},{8,11},{9,8},{10,9... | collective-permute-start | bytes 983048 | tf_op jit(solution)/shard_map/ppermute | solution.py:228
  38.5 10.3 %collective-permute-start = (bf16[320,512]{1,0:T(8,128)(2,1)S(1)}, bf16[320,512]{1,0:T(8,128)(2,1)S(1)}, u32[]{:S(2)}, u32[]{:S(2)}) collective-permute-start(bf16[320,512]{1,0:T(8,128)(2,1)S(1)} %get-tuple-element.26.refs_0_), channel_id=1, source_target_pairs={{0,1},{1,2},{2,3},{3,0},{4,5},{5,6},{6,7},{7,4},{8,9},{9,10},{10,1... | collective-permute-start | bytes 983048 | tf_op jit(solution)/shard_map/ppermute | solution.py:228
  44.3 15.8 %collective-permute-start.6 = (bf16[320,512]{1,0:T(8,128)(2,1)S(1)}, bf16[320,512]{1,0:T(8,128)(2,1)S(1)}, u32[]{:S(2)}, u32[]{:S(2)}) collective-permute-start(bf16[320,512]{1,0:T(8,128)(2,1)S(1)} %get-tuple-element.32.refs_0_), channel_id=1, source_target_pairs={{0,1},{1,2},{2,3},{3,0},{4,5},{5,6},{6,7},{7,4},{8,9},{9,10},{10,1... | collective-permute-start | bytes 983048 | tf_op jit(solution)/shard_map/ppermute | solution.py:228
  48.8 11.4 %collective-permute-start.8 = (bf16[320,512]{1,0:T(8,128)(2,1)S(1)}, bf16[320,512]{1,0:T(8,128)(2,1)S(1)}, u32[]{:S(2)}, u32[]{:S(2)}) collective-permute-start(bf16[320,512]{1,0:T(8,128)(2,1)S(1)} %collective-permute-done.7.refs_2_), channel_id=1, source_target_pairs={{0,3},{1,0},{2,1},{3,2},{4,7},{5,4},{6,5},{7,6},{8,11},{9,8},{10,9... | collective-permute-start | bytes 983048 | tf_op jit(solution)/shard_map/ppermute | solution.py:228
  53.3 17.6 %collective-permute-start.1 = (bf16[320,512]{1,0:T(8,128)(2,1)S(1)}, bf16[320,512]{1,0:T(8,128)(2,1)S(1)}, u32[]{:S(2)}, u32[]{:S(2)}) collective-permute-start(bf16[320,512]{1,0:T(8,128)(2,1)S(1)} %get-tuple-element.26.refs_0_), channel_id=1, source_target_pairs={{0,3},{1,0},{2,1},{3,2},{4,7},{5,4},{6,5},{7,6},{8,11},{9,8},{10,9... | collective-permute-start | bytes 983048 | tf_op jit(solution)/shard_map/ppermute | solution.py:228
  54.6 16.2 %collective-permute-start.2 = (bf16[320,512]{1,0:T(8,128)(2,1)S(1)}, bf16[320,512]{1,0:T(8,128)(2,1)S(1)}, u32[]{:S(2)}, u32[]{:S(2)}) collective-permute-start(bf16[320,512]{1,0:T(8,128)(2,1)S(1)} %collective-permute-done.refs_1_), channel_id=1, source_target_pairs={{0,1},{1,2},{2,3},{3,0},{4,5},{5,6},{6,7},{7,4},{8,9},{9,10},{10,1... | collective-permute-start | bytes 983048 | tf_op jit(solution)/shard_map/ppermute | solution.py:228
  68.6 11.0 %collective-permute-start.12 = (bf16[320,512]{1,0:T(8,128)(2,1)S(1)}, bf16[320,512]{1,0:T(8,128)(2,1)S(1)}, u32[]{:S(2)}, u32[]{:S(2)}) collective-permute-start(bf16[320,512]{1,0:T(8,128)(2,1)S(1)} %get-tuple-element.38), channel_id=1, source_target_pairs={{0,3},{1,0},{2,1},{3,2},{4,7},{5,4},{6,5},{7,6},{8,11},{9,8},{10,9... | collective-permute-start | bytes 983048 | tf_op jit(solution)/shard_map/ppermute | solution.py:228
  79.3 12.1 %collective-permute-start.9 = (bf16[320,512]{1,0:T(8,128)(2,1)S(1)}, bf16[320,512]{1,0:T(8,128)(2,1)S(1)}, u32[]{:S(2)}, u32[]{:S(2)}) collective-permute-start(bf16[320,512]{1,0:T(8,128)(2,1)S(1)} %get-tuple-element.35), channel_id=1, source_target_pairs={{0,1},{1,2},{2,3},{3,0},{4,5},{5,6},{6,7},{7,4},{8,9},{9,10},{10,1... | collective-permute-start | bytes 983048 | tf_op jit(solution)/shard_map/ppermute | solution.py:228
  79.7 21.2 %collective-permute-start.13 = (bf16[640,512]{1,0:T(8,128)(2,1)S(1)}, bf16[640,512]{1,0:T(8,128)(2,1)S(1)}, u32[]{:S(2)}, u32[]{:S(2)}) collective-permute-start(bf16[640,512]{1,0:T(8,128)(2,1)S(1)} %shard_map.80), channel_id=1, source_target_pairs={{0,3},{1,0},{2,1},{3,2},{4,7},{5,4},{6,5},{7,6},{8,11},{9,8},{10,9... | collective-permute-start | bytes 1966088 | tf_op jit(solution)/shard_map/ppermute | solution.py:228
  83.0 14.4 %collective-permute-start.11 = (bf16[320,512]{1,0:T(8,128)(2,1)S(1)}, bf16[320,512]{1,0:T(8,128)(2,1)S(1)}, u32[]{:S(2)}, u32[]{:S(2)}) collective-permute-start(bf16[320,512]{1,0:T(8,128)(2,1)S(1)} %get-tuple-element.36), channel_id=1, source_target_pairs={{0,1},{1,2},{2,3},{3,0},{4,5},{5,6},{6,7},{7,4},{8,9},{9,10},{10,1... | collective-permute-start | bytes 983048 | tf_op jit(solution)/shard_map/ppermute | solution.py:228
  91.4 9.4 %collective-permute-start.10 = (bf16[320,512]{1,0:T(8,128)(2,1)S(1)}, bf16[320,512]{1,0:T(8,128)(2,1)S(1)}, u32[]{:S(2)}, u32[]{:S(2)}) collective-permute-start(bf16[320,512]{1,0:T(8,128)(2,1)S(1)} %shard_map.79), channel_id=1, source_target_pairs={{0,1},{1,2},{2,3},{3,0},{4,5},{5,6},{6,7},{7,4},{8,9},{9,10},{10,1... | collective-permute-start | bytes 983048 | tf_op jit(solution)/shard_map/ppermute | solution.py:228
  102.3 23.0 %all-to-all-start.1 = ((bf16[32,80,128]{2,1,0:T(8,128)(2,1)}), bf16[32,80,128]{2,1,0:T(8,128)(2,1)S(1)}, u32[]{:S(2)}, u32[]{:S(2)}) async-start(bf16[32,80,128]{2,1,0:T(8,128)(2,1)} %shard_map.81), calls=%async_computation.1 | async-start | bytes 1310720 | tf_op jit(solution)/shard_map/all_to_all | solution.py:231
